TPU v7x, 32 devices: a whole 2x2x4 slice. The times are simulated.
32 devices in a mesh: fs: 8 (over z, x), tp: 4 (over y, core).
Axes of the slice: x: 2, y: 2, z: 4, core: 2. Of those that a mesh axis runs over, the one named last changes fastest.
Arguments:
- normed_inputs: bfloat16 [24576, 2048], P(('fs', 'tp')), may hold values from -6 to 6
- query_cotangent: bfloat16 [24576, 1024], P(('fs', 'tp')), may hold values from -6 to 6
- head_outputs: bfloat16 [24576, 1024], P(('fs', 'tp')), may hold values from -6 to 6
- output_cotangent: bfloat16 [24576, 2048], P(('fs', 'tp')), may hold values from -6 to 6
- query_weight: float32 [2048, 1024], P('fs', 'tp'), may hold values from -0.125 to 0.125
- out_weight: float32 [1024, 2048], P('fs', 'tp'), may hold values from -0.1875 to 0.1875
- query_basis: bfloat16 [2048, 512], P('fs'), may hold values from -0.125 to 0.125
- out_basis: bfloat16 [1024, 512], P('fs'), may hold values from -0.1875 to 0.1875
- query_mean: float32 [512, 1024], P('fs', 'tp'), may hold values from -6 to 6
- query_square: float32 [512, 1024], P('fs', 'tp'), may hold values from 0.5 to 2
- out_mean: float32 [512, 2048], P('fs', 'tp'), may hold values from -6 to 6
- out_square: float32 [512, 2048], P('fs', 'tp'), may hold values from 0.5 to 2
Outputs:
- query_mean_new: float32 [512, 1024], P('fs', 'tp')
- query_square_new: float32 [512, 1024], P('fs', 'tp')
- query_step: float32 [2048, 1024], P('fs', 'tp')
- query_weight_new: float32 [2048, 1024], P('fs', 'tp')
- query_copy: bfloat16 [2048, 1024], P(None, 'tp')
- out_mean_new: float32 [512, 2048], P('fs', 'tp')
- out_square_new: float32 [512, 2048], P('fs', 'tp')
- out_step: float32 [1024, 2048], P('fs', 'tp')
- out_weight_new: float32 [1024, 2048], P('fs', 'tp')
- out_copy: bfloat16 [1024, 2048], P(None, 'tp')
All inputs are finite; a program needn't handle non-finite values.
Results may differ from a plain program's by a relative error of at most 0.009.
Values may be sent and summed in bfloat16 or wider, within the bound.
No kernel may reach another device: no remote copies, remote signals or barrier semaphores. Data moves between devices by JAX's collectives and lax.ppermute only.
A program may use at most 64 MiB of HBM per device.

v0:
```python
import jax
import jax.numpy as jnp
from jax import lax
from jax.sharding import PartitionSpec as P


def moments(reduced, mean, square):
    mean_new = 0.8 * mean + 0.2 * reduced
    square_new = 0.9 * square + 0.1 * reduced * reduced
    direction = mean_new / (jnp.sqrt(square_new) + 1e-08)
    return (mean_new, square_new, direction)


def split_product(left, right):
    contract = (((0,), (0,)), ((), ()))
    high = left.astype(jnp.bfloat16)
    low = (left - high.astype(jnp.float32)).astype(jnp.bfloat16)
    return lax.dot_general(
        high, right, contract, preferred_element_type=jnp.float32
    ) + lax.dot_general(low, right, contract, preferred_element_type=jnp.float32)


def shards(
    normed_inputs,
    query_cotangent,
    head_outputs,
    output_cotangent,
    query_weight,
    out_weight,
    query_basis,
    out_basis,
    query_mean,
    query_square,
    out_mean,
    out_square,
):
    fs_count = lax.axis_size("fs")
    tp_count = lax.axis_size("tp")
    model_rows = normed_inputs.shape[1]
    query_width = query_cotangent.shape[1]
    token_scale = (normed_inputs.shape[0] * fs_count * tp_count) ** (-0.5)
    query_cols = query_weight.shape[1]
    out_cols = out_weight.shape[1]
    rank_rows = query_mean.shape[0]
    query_all, out_all = (
        lax.all_gather(query_basis, "fs", axis=0, tiled=True),
        lax.all_gather(out_basis, "fs", axis=0, tiled=True),
    )
    query_left = jnp.dot(normed_inputs, query_all, preferred_element_type=jnp.float32)
    out_left = jnp.dot(head_outputs, out_all, preferred_element_type=jnp.float32)
    query_part = split_product(query_left, query_cotangent)
    out_part = split_product(out_left, output_cotangent)
    reduced = lax.psum_scatter(
        jnp.concatenate(
            [
                query_part.reshape(rank_rows * lax.axis_size("fs"), tp_count, query_cols),
                out_part.reshape(rank_rows * lax.axis_size("fs"), tp_count, out_cols),
            ],
            axis=2,
        ).astype(jnp.bfloat16),
        "fs",
        scatter_dimension=0,
        tiled=True,
    )
    summed = lax.psum_scatter(reduced, "tp", scatter_dimension=1, tiled=True).astype(jnp.float32)
    projected = summed[:, 0, :]
    projected = projected * token_scale
    query_reduced = projected[:, :query_cols]
    out_reduced = projected[:, query_cols:]
    query_mean_new, query_square_new, query_direction = moments(
        query_reduced, query_mean, query_square
    )
    out_mean_new, out_square_new, out_direction = moments(out_reduced, out_mean, out_square)
    query_piece = lax.all_gather(query_direction, "fs", axis=0, tiled=True)
    out_piece = lax.all_gather(out_direction, "fs", axis=0, tiled=True)
    query_part = query_basis.astype(jnp.float32)
    out_part = out_basis.astype(jnp.float32)
    query_full = jnp.dot(query_part, query_piece, precision=lax.Precision.HIGHEST)
    out_full = jnp.dot(out_part, out_piece, precision=lax.Precision.HIGHEST)
    query_norms, out_norms = lax.psum(
        (jnp.sum(query_full * query_full, axis=0), jnp.sum(out_full * out_full, axis=0)), "fs"
    )
    query_step = query_full * lax.rsqrt(query_norms / model_rows + 0.05)
    out_step = out_full * lax.rsqrt(out_norms / query_width + 0.05)
    query_weight_new = query_weight - 0.01 * query_step
    out_weight_new = out_weight - 0.01 * out_step
    query_copy, out_copy = (
        lax.all_gather(query_weight_new.astype(jnp.bfloat16), "fs", axis=0, tiled=True),
        lax.all_gather(out_weight_new.astype(jnp.bfloat16), "fs", axis=0, tiled=True),
    )
    return (
        query_mean_new,
        query_square_new,
        query_step,
        query_weight_new,
        query_copy,
        out_mean_new,
        out_square_new,
        out_step,
        out_weight_new,
        out_copy,
    )


def solution(mesh):
    in_specs = (
        P(("fs", "tp"), None),
        P(("fs", "tp"), None),
        P(("fs", "tp"), None),
        P(("fs", "tp"), None),
        P("fs", "tp"),
        P("fs", "tp"),
        P("fs", None),
        P("fs", None),
        P("fs", "tp"),
        P("fs", "tp"),
        P("fs", "tp"),
        P("fs", "tp"),
    )
    out_specs = (
        P("fs", "tp"),
        P("fs", "tp"),
        P("fs", "tp"),
        P("fs", "tp"),
        P(None, "tp"),
        P("fs", "tp"),
        P("fs", "tp"),
        P("fs", "tp"),
        P("fs", "tp"),
        P(None, "tp"),
    )
    return jax.shard_map(shards, mesh=mesh, in_specs=in_specs, out_specs=out_specs, check_vma=False)
```

profile of v0, /device:TPU:0, one launch (start us, length us, event | category | flops | bytes accessed | tf_op | source)
XLA Modules:
  0.0 366.5 jit_solution(16840274893185502602)
XLA Ops:
  8.7 44.4 %all-gather.8.cloned.1.call-done = bf16[1024,512]{1,0:T(8,128)(2,1)} async-done(((bf16[128,512]{1,0:T(8,128)(2,1)}), bf16[1024,512]{1,0:T(8,128)(2,1)}) %all-gather.8.cloned.1.call-update) | async-done | bytes 1048592 | tf_op jit(solution)/shard_map/all_gather | solution.py:47
  53.2 2.7 fusion.13
  55.8 1.8 fusion.1
  57.7 1.8 add_convert_fusion
  59.5 1.5 copy.28
  61.0 42.1 %all-gather.6.cloned.1.call-done = bf16[2048,512]{1,0:T(8,128)(2,1)} async-done(((bf16[256,512]{1,0:T(8,128)(2,1)}), bf16[2048,512]{1,0:T(8,128)(2,1)}) %all-gather.6.cloned.1.call-update) | async-done | bytes 2097168 | tf_op jit(solution)/shard_map/all_gather | solution.py:46
  103.1 4.4 %fusion.12 = f32[768,512]{1,0:T(8,128)S(1)} fusion(bf16[768,2048]{1,0:T(8,128)(2,1)} %param.12, bf16[2048,512]{1,0:T(8,128)(2,1)} %all-gather.6.cloned.1.call-done), kind=kOutput, calls=%fused_computation.32 | convolution fusion | flops 1610612736 | bytes 6815744 | tf_op jit(solution)/shard_map/dot_general | solution.py:49
  108.6 1.0 add_convert_fusion.1
  109.7 1.5 copy-done.1
  111.2 1.9 pad_maximum_fusion
  113.1 73.1 %reduce-scatter.3.cloned.1.call-done = bf16[64,4,768]{2,0,1:T(8,128)(2,1)} async-done(((bf16[512,4,768]{2,0,1:T(8,128)(2,1)}), bf16[64,4,768]{2,0,1:T(8,128)(2,1)}) %reduce-scatter.3.cloned.1.call-update) | async-done | bytes 393232 | tf_op jit(solution)/shard_map/reduce_scatter | solution.py:53
  186.3 22.2 %reduce-scatter.5.cloned.1.call-done = bf16[64,1,768]{2,0,1:T(8,128)(2,1)} async-done(((bf16[64,4,768]{2,0,1:T(8,128)(2,1)}), bf16[64,1,768]{2,0,1:T(8,128)(2,1)}) %reduce-scatter.5.cloned.1.call-update) | async-done | bytes 98320 | tf_op jit(solution)/shard_map/reduce_scatter | solution.py:65
  210.1 1.7 add_divide_fusion
  211.9 1.6 add_divide_fusion.1
  213.5 32.6 %all_gather.20 = f32[512,256]{1,0:T(8,128)S(1)} all-gather(f32[64,256]{1,0:T(8,128)S(1)} %get-tuple-element.21), channel_id=1, replica_groups=mesh['fs'=8,'tp'=4] {'fs'}, dimensions={0}, use_global_device_ids=true | all-gather | bytes 589824 | tf_op jit(solution)/shard_map/all_gather | solution.py:74
  246.1 1.1 multiply_reduce_fusion.1
  247.2 6.5 %all-gather.12.cloned.1.call-done = f32[512,512]{1,0:T(8,128)} async-done(((f32[64,512]{1,0:T(8,128)}), f32[512,512]{1,0:T(8,128)}) %all-gather.12.cloned.1.call-update) | async-done | bytes 1048592 | tf_op jit(solution)/shard_map/all_gather | solution.py:75
  253.7 2.4 multiply_reduce_fusion
  256.2 19.1 %all-reduce = (f32[256]{0:T(256)S(1)}, f32[512]{0:T(512)S(1)}) all-reduce(f32[256]{0:T(256)S(1)} %get-tuple-element.24, f32[512]{0:T(512)S(1)} %get-tuple-element.26), channel_id=1, replica_groups=mesh['fs'=8,'tp'=4] {'fs'}, use_global_device_ids=true, to_apply=%region_3.0 | all-reduce | flops 768 | bytes 6144 | tf_op jit(solution)/shard_map/psum | solution.py:80
  275.2 1.9 fusion.8
  277.3 1.8 fusion.9
  279.1 35.5 %all-gather.14.cloned.1.call-done = bf16[1024,512]{1,0:T(8,128)(2,1)} async-done(((bf16[128,512]{1,0:T(8,128)(2,1)}), bf16[1024,512]{1,0:T(8,128)(2,1)}) %all-gather.14.cloned.1.call-update) | async-done | bytes 1048592 | tf_op jit(solution)/shard_map/all_gather | solution.py:89
  314.7 41.7 %all-gather.10.cloned.1.call-done = bf16[2048,256]{1,0:T(8,128)(2,1)} async-done(((bf16[256,256]{1,0:T(8,128)(2,1)}), bf16[2048,256]{1,0:T(8,128)(2,1)}) %all-gather.10.cloned.1.call-update) | async-done | bytes 1048592 | tf_op jit(solution)/shard_map/all_gather | solution.py:88
  356.4 2.4 copy.32
  (35 shorter events, 5.4 us)
Async XLA Ops:
  7.2 48.7 %copy-start = (bf16[768,2048]{1,0:T(8,128)(2,1)S(1)}, bf16[768,2048]{1,0:T(8,128)(2,1)}, u32[]{:S(2)}) copy-start(bf16[768,2048]{1,0:T(8,128)(2,1)} %param.15) | copy-start | bytes 9437188
  7.2 46.0 %all-gather.8.cloned.1.call-start = ((), (), s32[]{:S(2)}) async-start(), calls=%async_computation.3 | async-start | bytes 1179648 | tf_op jit(solution)/shard_map/all_gather | solution.py:47
  7.9 95.2 %all-gather.6.cloned.1.call-start = ((), (), s32[]{:S(2)}) async-start(), calls=%async_computation.2 | async-start | bytes 2359296 | tf_op jit(solution)/shard_map/all_gather | solution.py:46
  8.7 177.5 %reduce-scatter.3.cloned.1.call-start = ((), (), s32[]{:S(2)}) async-start(), calls=%async_computation.4 | async-start | bytes 3538944 | tf_op jit(solution)/shard_map/reduce_scatter | solution.py:53
  103.1 4.4 %copy-start.7 = (bf16[768,1024]{1,0:T(8,128)(2,1)S(1)}, bf16[768,1024]{1,0:T(8,128)(2,1)}, u32[]{:S(2)}) copy-start(bf16[768,1024]{1,0:T(8,128)(2,1)} %param.13) | copy-start | bytes 4718596
  109.6 1.6 copy-start.1
  113.0 133.0 %copy-start.2 = (bf16[256,512]{1,0:T(8,128)(2,1)S(1)}, bf16[256,512]{1,0:T(8,128)(2,1)}, u32[]{:S(2)}) copy-start(bf16[256,512]{1,0:T(8,128)(2,1)} %param.18) | copy-start | bytes 786436
  113.1 140.7 %copy-start.6 = (bf16[128,512]{1,0:T(8,128)(2,1)S(1)}, bf16[128,512]{1,0:T(8,128)(2,1)}, u32[]{:S(2)}) copy-start(bf16[128,512]{1,0:T(8,128)(2,1)} %param.19) | copy-start | bytes 393220
  113.1 95.4 %reduce-scatter.5.cloned.1.call-start = ((), (), s32[]{:S(2)}) async-start(), calls=%async_computation.5 | async-start | bytes 491520 | tf_op jit(solution)/shard_map/reduce_scatter | solution.py:65
  186.2 67.5 %all-gather.12.cloned.1.call-start = ((), (), s32[]{:S(2)}) async-start(), calls=%async_computation.7 | async-start | bytes 1179648 | tf_op jit(solution)/shard_map/all_gather | solution.py:75
  209.4 0.7 copy-start.5
  211.9 102.8 %all-gather.14.cloned.1.call-start = ((), (), s32[]{:S(2)}) async-start(), calls=%async_computation.8 | async-start | bytes 1179648 | tf_op jit(solution)/shard_map/all_gather | solution.py:89
  247.2 30.1 %copy-start.4 = (f32[256,256]{0,1:T(8,128)S(1)}, f32[256,256]{0,1:T(8,128)}, u32[]{:S(2)}) copy-start(f32[256,256]{0,1:T(8,128)} %get-tuple-element.25) | copy-start | bytes 786436
  277.2 79.2 %all-gather.10.cloned.1.call-start = ((), (), s32[]{:S(2)}) async-start(), calls=%async_computation.6 | async-start | bytes 1179648 | tf_op jit(solution)/shard_map/all_gather | solution.py:88
  356.4 2.4 copy-start.3
Sparse Core Ops, SparseCore 0:
  10.1 42.9 all-gather.7
  55.3 47.7 all-gather.5
  113.2 72.9 reduce-scatter.2
  188.5 19.9 reduce-scatter.4
  212.0 41.7 all-gather.11
  277.3 37.2 all-gather.13
  317.3 38.9 all-gather.9
where the time goes:
time: 367 us
  waiting for transfers between devices  267 us (73%)
  blocking collectives  51.6 us (14%)
  matrix products  16.4 us (4%)
  between operations  14.2 us (4%)
  other arithmetic  9.87 us (3%)
  local copies, waits for them, and re-layouts  7.1 us (2%)
    reduce_scatter x1, waiting for transfers between devices, shards(): lax.psum_scatter(jnp.concatenate([query_part.reshape(rank_rows * lax.axis...  73.1 us
    all_gather x1, waiting for transfers between devices, shards(): lax.all_gather(out_basis, 'fs', axis=0, tiled=True)  44.4 us
    all_gather x1, waiting for transfers between devices, shards(): lax.all_gather(query_basis, 'fs', axis=0, tiled=True)  42.1 us
    all_gather x1, waiting for transfers between devices, shards(): lax.all_gather(query_weight_new.astype(jnp.bfloat16), 'fs', axis=0, tiled...  41.7 us
    all_gather x1, waiting for transfers between devices, shards(): lax.all_gather(out_weight_new.astype(jnp.bfloat16), 'fs', axis=0, tiled=T...  35.5 us
    all_gather x1, blocking collectives, shards(): query_piece = lax.all_gather(query_direction, 'fs', axis=0, tiled=True)  32.6 us
    reduce_scatter x1, waiting for transfers between devices, shards(): lax.psum_scatter(reduced, 'tp', scatter_dimension=1, tiled=True)  22.2 us
    psum x1, blocking collectives, shards(): lax.psum((jnp.sum(query_full * query_full, axis=0), jnp.sum(out_full * ou...  19.1 us
  transfers between devices with their start and end apart: 7, of which 7 were waited for; matrix products, arithmetic and copies ran while one was open for 3% of the time, Pallas kernels for 0%

commit v1 on v0

--- a/solution.py
+++ b/solution.py
@@ -2,6 +2,12 @@
 import jax.numpy as jnp
 from jax import lax
 from jax.sharding import PartitionSpec as P
+
+draft_blocks = lambda q_in, local_x, dev_axis: jnp.split(
+    jax.lax.all_gather(jnp.concatenate([q_in, local_x], 1), dev_axis, axis=0, tiled=True),
+    [q_in.shape[1]],
+    1,
+)
 
 
 def moments(reduced, mean, square):
@@ -71,8 +77,7 @@
         query_reduced, query_mean, query_square
     )
     out_mean_new, out_square_new, out_direction = moments(out_reduced, out_mean, out_square)
-    query_piece = lax.all_gather(query_direction, "fs", axis=0, tiled=True)
-    out_piece = lax.all_gather(out_direction, "fs", axis=0, tiled=True)
+    query_piece, out_piece = draft_blocks(query_direction, local_x=out_direction, dev_axis="fs")
     query_part = query_basis.astype(jnp.float32)
     out_part = out_basis.astype(jnp.float32)
     query_full = jnp.dot(query_part, query_piece, precision=lax.Precision.HIGHEST)

time: 367 us -> 373 us (1.016)
  waiting for transfers between devices: 267 us -> 305 us
  blocking collectives: 51.6 us -> 18.8 us
    all_gather x1, waiting for transfers between devices: 6.53 us -> 44.3 us  [jax.lax.all_gather(jnp.concatenate([q_in, local_x], 1), dev_axis, axis=0,...]
    all_gather x1 -> x0, blocking collectives: 32.6 us -> none  [shards(): query_piece = lax.all_gather(query_direction, 'fs', axis=0, tiled=True)]
where the time goes in v1:
time: 373 us
  waiting for transfers between devices  305 us (82%)
  blocking collectives  18.8 us (5%)
  matrix products  17.4 us (5%)
  between operations  14.2 us (4%)
  other arithmetic  10.6 us (3%)
  local copies, waits for them, and re-layouts  6.44 us (2%)
    reduce_scatter x1, waiting for transfers between devices, shards(): lax.psum_scatter(jnp.concatenate([query_part.reshape(rank_rows * lax.axis...  73.1 us
    all_gather x1, waiting for transfers between devices, shards(): lax.all_gather(out_basis, 'fs', axis=0, tiled=True)  44.4 us
    all_gather x1, waiting for transfers between devices, jax.lax.all_gather(jnp.concatenate([q_in, local_x], 1), dev_axis, axis=0,...  44.3 us
    all_gather x1, waiting for transfers between devices, shards(): lax.all_gather(query_basis, 'fs', axis=0, tiled=True)  42.1 us
    all_gather x1, waiting for transfers between devices, shards(): lax.all_gather(query_weight_new.astype(jnp.bfloat16), 'fs', axis=0, tiled...  41.7 us
    all_gather x1, waiting for transfers between devices, shards(): lax.all_gather(out_weight_new.astype(jnp.bfloat16), 'fs', axis=0, tiled=T...  35.7 us
    reduce_scatter x1, waiting for transfers between devices, shards(): lax.psum_scatter(reduced, 'tp', scatter_dimension=1, tiled=True)  22.2 us
    psum x1, blocking collectives, shards(): lax.psum((jnp.sum(query_full * query_full, axis=0), jnp.sum(out_full * ou...  18.8 us
  transfers between devices with their start and end apart: 7, of which 7 were waited for; matrix products, arithmetic and copies ran while one was open for 3% of the time, Pallas kernels for 0%

profile of v1, /device:TPU:0, one launch (start us, length us, event | category | flops | bytes accessed | tf_op | source)
XLA Modules:
  0.0 372.6 jit_solution(12111795478647899167)
XLA Ops:
  8.7 44.4 %all-gather.8.cloned.1.call-done = bf16[1024,512]{1,0:T(8,128)(2,1)} async-done(((bf16[128,512]{1,0:T(8,128)(2,1)}), bf16[1024,512]{1,0:T(8,128)(2,1)}) %all-gather.8.cloned.1.call-update) | async-done | bytes 1048592 | tf_op jit(solution)/shard_map/all_gather | solution.py:53
  53.2 2.7 fusion.17
  55.8 1.8 fusion.5
  57.7 1.8 add_convert_fusion
  59.5 1.5 copy.28
  61.0 42.1 %all-gather.6.cloned.1.call-done = bf16[2048,512]{1,0:T(8,128)(2,1)} async-done(((bf16[256,512]{1,0:T(8,128)(2,1)}), bf16[2048,512]{1,0:T(8,128)(2,1)}) %all-gather.6.cloned.1.call-update) | async-done | bytes 2097168 | tf_op jit(solution)/shard_map/all_gather | solution.py:52
  103.1 4.4 %fusion.16 = f32[768,512]{1,0:T(8,128)S(1)} fusion(bf16[768,2048]{1,0:T(8,128)(2,1)} %param.12, bf16[2048,512]{1,0:T(8,128)(2,1)} %all-gather.6.cloned.1.call-done), kind=kOutput, calls=%fused_computation.37 | convolution fusion | flops 1610612736 | bytes 6815744 | tf_op jit(solution)/shard_map/dot_general | solution.py:55
  107.6 1.0 fusion.8
  108.6 1.0 add_convert_fusion.1
  109.7 1.5 copy-done.1
  111.2 1.8 pad_maximum_fusion
  113.1 73.1 %reduce-scatter.3.cloned.1.call-done = bf16[64,4,768]{2,0,1:T(8,128)(2,1)} async-done(((bf16[512,4,768]{2,0,1:T(8,128)(2,1)}), bf16[64,4,768]{2,0,1:T(8,128)(2,1)}) %reduce-scatter.3.cloned.1.call-update) | async-done | bytes 393232 | tf_op jit(solution)/shard_map/reduce_scatter | solution.py:59
  186.3 22.2 %reduce-scatter.5.cloned.1.call-done = bf16[64,1,768]{2,0,1:T(8,128)(2,1)} async-done(((bf16[64,4,768]{2,0,1:T(8,128)(2,1)}), bf16[64,1,768]{2,0,1:T(8,128)(2,1)}) %reduce-scatter.5.cloned.1.call-update) | async-done | bytes 98320 | tf_op jit(solution)/shard_map/reduce_scatter | solution.py:71
  209.4 1.7 add_divide_fusion
  211.1 1.6 add_divide_fusion.1
  213.5 44.3 %all-gather.10.cloned.1.call-done = f32[512,768]{1,0:T(8,128)} async-done(((f32[64,768]{1,0:T(8,128)}), f32[512,768]{1,0:T(8,128)}) %all-gather.10.cloned.1.call-update) | async-done | bytes 1572880 | tf_op jit(solution)/shard_map/all_gather | solution.py:7
  257.7 2.4 multiply_reduce_fusion
  260.2 2.2 multiply_reduce_fusion.1
  262.3 18.8 %all-reduce = (f32[256]{0:T(256)S(1)}, f32[512]{0:T(512)S(1)}) all-reduce(f32[256]{0:T(256)S(1)} %get-tuple-element.24, f32[512]{0:T(512)S(1)} %get-tuple-element.26), channel_id=1, replica_groups=mesh['fs'=8,'tp'=4] {'fs'}, use_global_device_ids=true, to_apply=%region_3.0 | all-reduce | flops 768 | bytes 6144 | tf_op jit(solution)/shard_map/psum | solution.py:85
  281.1 1.9 fusion.12
  283.2 1.9 fusion.13
  285.1 35.7 %all-gather.14.cloned.1.call-done = bf16[1024,512]{1,0:T(8,128)(2,1)} async-done(((bf16[128,512]{1,0:T(8,128)(2,1)}), bf16[1024,512]{1,0:T(8,128)(2,1)}) %all-gather.14.cloned.1.call-update) | async-done | bytes 1048592 | tf_op jit(solution)/shard_map/all_gather | solution.py:94
  320.8 41.7 %all-gather.12.cloned.1.call-done = bf16[2048,256]{1,0:T(8,128)(2,1)} async-done(((bf16[256,256]{1,0:T(8,128)(2,1)}), bf16[2048,256]{1,0:T(8,128)(2,1)}) %all-gather.12.cloned.1.call-update) | async-done | bytes 1048592 | tf_op jit(solution)/shard_map/all_gather | solution.py:93
  362.5 2.4 copy.32
  (31 shorter events, 4.4 us)
Async XLA Ops:
  7.2 48.7 %copy-start = (bf16[768,2048]{1,0:T(8,128)(2,1)S(1)}, bf16[768,2048]{1,0:T(8,128)(2,1)}, u32[]{:S(2)}) copy-start(bf16[768,2048]{1,0:T(8,128)(2,1)} %param.15) | copy-start | bytes 9437188
  7.2 46.0 %all-gather.8.cloned.1.call-start = ((), (), s32[]{:S(2)}) async-start(), calls=%async_computation.3 | async-start | bytes 1179648 | tf_op jit(solution)/shard_map/all_gather | solution.py:53
  7.9 95.2 %all-gather.6.cloned.1.call-start = ((), (), s32[]{:S(2)}) async-start(), calls=%async_computation.2 | async-start | bytes 2359296 | tf_op jit(solution)/shard_map/all_gather | solution.py:52
  8.7 177.5 %reduce-scatter.3.cloned.1.call-start = ((), (), s32[]{:S(2)}) async-start(), calls=%async_computation.4 | async-start | bytes 3538944 | tf_op jit(solution)/shard_map/reduce_scatter | solution.py:59
  103.1 4.4 %copy-start.5 = (bf16[768,1024]{1,0:T(8,128)(2,1)S(1)}, bf16[768,1024]{1,0:T(8,128)(2,1)}, u32[]{:S(2)}) copy-start(bf16[768,1024]{1,0:T(8,128)(2,1)} %param.13) | copy-start | bytes 4718596
  109.6 1.6 copy-start.1
  113.0 144.7 %copy-start.4 = (bf16[128,512]{1,0:T(8,128)(2,1)S(1)}, bf16[128,512]{1,0:T(8,128)(2,1)}, u32[]{:S(2)}) copy-start(bf16[128,512]{1,0:T(8,128)(2,1)} %param.19) | copy-start | bytes 393220
  113.1 147.1 %copy-start.2 = (bf16[256,512]{1,0:T(8,128)(2,1)S(1)}, bf16[256,512]{1,0:T(8,128)(2,1)}, u32[]{:S(2)}) copy-start(bf16[256,512]{1,0:T(8,128)(2,1)} %param.18) | copy-start | bytes 786436
  113.1 95.4 %reduce-scatter.5.cloned.1.call-start = ((), (), s32[]{:S(2)}) async-start(), calls=%async_computation.5 | async-start | bytes 491520 | tf_op jit(solution)/shard_map/reduce_scatter | solution.py:71
  186.2 71.5 %all-gather.10.cloned.1.call-start = ((), (), s32[]{:S(2)}) async-start(), calls=%async_computation.6 | async-start | bytes 1769472 | tf_op jit(solution)/shard_map/all_gather | solution.py:7
  213.4 107.3 %all-gather.14.cloned.1.call-start = ((), (), s32[]{:S(2)}) async-start(), calls=%async_computation.8 | async-start | bytes 1179648 | tf_op jit(solution)/shard_map/all_gather | solution.py:94
  283.1 79.4 %all-gather.12.cloned.1.call-start = ((), (), s32[]{:S(2)}) async-start(), calls=%async_computation.7 | async-start | bytes 1179648 | tf_op jit(solution)/shard_map/all_gather | solution.py:93
  362.5 2.4 copy-start.3
Sparse Core Ops, SparseCore 0:
  10.1 42.9 all-gather.7
  55.3 47.7 all-gather.5
  113.2 72.9 reduce-scatter.2
  188.5 19.9 reduce-scatter.4
  213.5 44.1 all-gather.9
  283.2 37.4 all-gather.13
  323.5 38.9 all-gather.11
